TPU v7x, 32 devices: a whole 2x2x4 slice. The times are simulated.
32 devices in a mesh: fs: 16 (over z, y, x), tp: 2 (over core).
Axes of the slice: x: 2, y: 2, z: 4, core: 2. Of those that a mesh axis runs over, the one named last changes fastest.
Arguments:
- sequence_entries: bfloat16 [4096, 2048], P('fs', 'tp'), may hold values from -6 to 6
- former_norm_factor: float32 [2048], replicated, may hold values from 0.1 to 1.9
- conveyor_matrix: float32 [2048, 1536], P('fs', 'tp'), may hold values from -0.125 to 0.125
- conveyor_rescalers: float32 [1536], P('tp'), may hold values from 0.3 to 3
- blend_value_matrix: float32 [2048, 1536], P('fs', 'tp'), may hold values from -0.125 to 0.125
- blend_rescalers: float32 [1536], P('tp'), may hold values from 0.18 to 4.8, as said below
- blend_norm_factor: float32 [1536], P('tp'), may hold values from 0.1 to 1.9
- location_matrices: bfloat16 [24, 128, 128], P('tp'), may hold values from -0.5 to 0.5
- location_offsets: float32 [24, 128], P('tp'), may hold values from 0.1 to 1.9
- branch_emission_matrix: float32 [1536, 2048], P('tp', 'fs'), may hold values from -0.15625 to 0.15625
- emission_rescalers: float32 [2048], P('fs'), may hold values from 0.3 to 3
- latter_norm_factor: float32 [2048], replicated, may hold values from 0.1 to 1.9
- valve_matrix: float32 [2048, 5632], P('fs', 'tp'), may hold values from -0.125 to 0.125
- valve_rescalers: float32 [5632], P('tp'), may hold values from 0.3 to 3
- raising_matrix: float32 [2048, 5632], P('fs', 'tp'), may hold values from -0.125 to 0.125
- raising_rescalers: float32 [5632], P('tp'), may hold values from 0.3 to 3
- lowering_matrix: float32 [5632, 2048], P('tp', 'fs'), may hold values from -0.078125 to 0.078125
- lowering_rescalers: float32 [2048], P('fs'), may hold values from 0.3 to 3
Outputs:
- layer_out: bfloat16 [4096, 2048], P('fs', 'tp')
Inputs may be any that keep to these rules, and one draw needn't show every extreme that they name: `blend_rescalers`: positive column scales.
All inputs are finite; a program needn't handle non-finite values.
Results may differ from a plain program's by a relative error of at most 0.02.
Values may be sent and summed in bfloat16 or wider, within the bound.
A program may use at most 128 MiB of HBM per device.

v0:
```python
import jax
import jax.numpy as jnp
from jax import lax
from jax.sharding import PartitionSpec as P

EPS = 1e-06


def normalize(rows, gain):
    values = rows.astype(jnp.float32)
    factor = lax.rsqrt(jnp.mean(values * values, axis=-1, keepdims=True) + EPS)
    return (values * factor * gain).astype(jnp.bfloat16)


def elementwise_plus(left_rows, pieces):
    return (
        jnp.dot(left_rows, pieces[0], preferred_element_type=jnp.float32),
        jnp.dot(left_rows, pieces[1], preferred_element_type=jnp.float32),
    )


def project_cols(left_rows, scales, piece):
    return jnp.dot(left_rows, piece, preferred_element_type=jnp.float32) * scales


def on_device(
    sequence_entries,
    former_norm_factor,
    conveyor_matrix,
    conveyor_rescalers,
    blend_value_matrix,
    blend_rescalers,
    blend_norm_factor,
    location_matrices,
    location_offsets,
    branch_emission_matrix,
    emission_rescalers,
    latter_norm_factor,
    valve_matrix,
    valve_rescalers,
    raising_matrix,
    raising_rescalers,
    lowering_matrix,
    lowering_rescalers,
):
    out_scales, down_scales = (
        lax.all_gather(emission_rescalers, "fs", axis=0, tiled=True),
        lax.all_gather(lowering_rescalers, "fs", axis=0, tiled=True),
    )
    full_rows = lax.all_gather(sequence_entries, "tp", axis=1, tiled=True)
    own_width = sequence_entries.shape[1]
    own_start = lax.axis_index("tp") * own_width
    standardized_source = normalize(full_rows, former_norm_factor)
    conveyor_prior, stream_prior = elementwise_plus(
        standardized_source,
        (
            lax.all_gather(conveyor_matrix.astype(jnp.bfloat16), "fs", axis=0, tiled=True),
            lax.all_gather(blend_value_matrix.astype(jnp.bfloat16), "fs", axis=0, tiled=True),
        ),
    )
    conveyor_current = jax.nn.gelu(conveyor_prior * conveyor_rescalers)
    signal = jax.nn.gelu(stream_prior * blend_rescalers)
    total_sq = lax.psum(jnp.sum(signal * signal, axis=1), "tp")
    channels = signal.shape[1] * lax.axis_size("tp")
    signal_norm = (
        signal * lax.rsqrt(total_sq / channels + EPS)[:, None] * blend_norm_factor
    ).astype(jnp.bfloat16)
    local_groups = location_matrices.shape[0]
    block_len = location_matrices.shape[1]
    group_width = signal.shape[1] // local_groups
    lower_mask = jnp.tril(jnp.ones((block_len, block_len), bool))
    masked = jnp.where(lower_mask[None], location_matrices, jnp.zeros((), jnp.bfloat16))
    signal_blocks = signal_norm.reshape(-1, block_len, local_groups, group_width)
    location_blended = jnp.einsum(
        "gts,bsgd->btgd", masked, signal_blocks, preferred_element_type=jnp.float32
    )
    location_blended = location_blended + location_offsets.T[None, :, :, None]
    filtered_result = (conveyor_current * location_blended.reshape(conveyor_current.shape)).astype(
        jnp.bfloat16
    )
    mixer_terms = project_cols(
        filtered_result,
        out_scales,
        lax.all_gather(branch_emission_matrix.astype(jnp.bfloat16), "fs", axis=1, tiled=True),
    )
    summed = lax.psum(mixer_terms.astype(jnp.bfloat16), "tp").astype(jnp.float32)
    mid_rows = (full_rows.astype(jnp.float32) + summed).astype(jnp.bfloat16)
    mid_own = lax.dynamic_slice_in_dim(mid_rows, own_start, own_width, 1)
    ffn_in = normalize(mid_rows, latter_norm_factor)
    gate_half = valve_matrix.astype(jnp.bfloat16)
    up_half = raising_matrix.astype(jnp.bfloat16)
    whole_gate, whole_up = (
        lax.all_gather(gate_half, "fs", axis=0, tiled=True),
        lax.all_gather(up_half, "fs", axis=0, tiled=True),
    )
    pre_gate = jnp.dot(ffn_in, whole_gate, preferred_element_type=jnp.float32)
    pre_up = jnp.dot(ffn_in, whole_up, preferred_element_type=jnp.float32)
    hidden = (jax.nn.silu(pre_gate * valve_rescalers) * (pre_up * raising_rescalers)).astype(
        jnp.bfloat16
    )
    ffn_terms = project_cols(
        hidden,
        down_scales,
        lax.all_gather(lowering_matrix.astype(jnp.bfloat16), "fs", axis=1, tiled=True),
    )
    ffn_share = lax.psum_scatter(
        ffn_terms.astype(jnp.bfloat16), "tp", scatter_dimension=1, tiled=True
    ).astype(jnp.float32)
    return (mid_own.astype(jnp.float32) + ffn_share).astype(jnp.bfloat16)


def solution(mesh):
    return jax.shard_map(
        on_device,
        mesh=mesh,
        in_specs=(
            P("fs", "tp"),
            P(),
            P("fs", "tp"),
            P("tp"),
            P("fs", "tp"),
            P("tp"),
            P("tp"),
            P("tp", None, None),
            P("tp", None),
            P("tp", "fs"),
            P("fs"),
            P(),
            P("fs", "tp"),
            P("tp"),
            P("fs", "tp"),
            P("tp"),
            P("tp", "fs"),
            P("fs"),
        ),
        out_specs=P("fs", "tp"),
        check_vma=False,
    )
```

profile of v0, /device:TPU:0, one launch (start us, length us, event | category | flops | bytes accessed | tf_op | source)
XLA Modules:
  0.0 764.5 jit_solution(3299104337699982424)
XLA Ops:
  6.5 0.0 all-gather.10.cloned.1.call-start
  6.5 0.7 all-gather.10.cloned.1.call-update
  7.3 0.0 all-gather.14.cloned.1.call-start
  7.3 1.7 convert_element_type.64
  9.0 0.0 all-gather.14.cloned.1.call-update
  9.0 0.0 all-gather.12.cloned.1.call-start
  9.1 1.7 convert_element_type.63
  10.8 0.0 all-gather.12.cloned.1.call-update
  10.8 0.0 all-gather.16.cloned.1.call-start
  10.9 1.7 convert_element_type.67
  12.5 0.0 all-gather.16.cloned.1.call-update
  12.6 0.0 all-reduce.2.cloned.1.call-start
  12.6 0.0 copy-done.6
  12.6 42.5 %all-gather = f32[16,1,128]{2,1,0:T(1,128)S(1)} all-gather(f32[1,1,128]{2,1,0:T(1,128)S(1)} %bitcast.34), channel_id=1, replica_groups=mesh['fs'=16,'tp'=2] {'fs'}, dimensions={0}, use_global_device_ids=true | all-gather | bytes 8704 | tf_op jit(solution)/shard_map/all_gather | solution.py:47
  55.1 0.0 all-gather.10.cloned.1.call-done
  55.1 1.5 fusion.7
  56.7 0.0 copy-start.5
  56.7 0.0 copy-start.4
  56.7 35.8 %all-gather.14.cloned.1.call-done = bf16[2048,768]{1,0:T(8,128)(2,1)} async-done(((bf16[128,768]{1,0:T(8,128)(2,1)}), bf16[2048,768]{1,0:T(8,128)(2,1)}) %all-gather.14.cloned.1.call-update) | async-done | bytes 3145744 | tf_op jit(solution)/shard_map/all_gather | solution.py:58
  92.5 0.0 copy-done.10
  92.5 0.0 copy-done.12
  92.5 3.5 multiply_reduce_fusion
  96.0 0.0 copy-start.3
  96.0 2.6 psum.14
  98.6 0.0 copy-done.5
  98.6 0.1 multiply_convert_fusion
  98.8 0.2 copy.25
  99.0 0.1 reshape.40
  99.1 0.0 copy-done.4
  99.1 0.0 copy-done.3
  99.1 0.0 copy-start.13
  99.1 0.4 fusion.11
  99.5 0.6 copy.27
  100.1 0.1 copy.34
  100.2 0.3 copy.28
  100.4 61.3 %all-gather.12.cloned.1.call-done = bf16[2048,768]{1,0:T(8,128)(2,1)} async-done(((bf16[128,768]{1,0:T(8,128)(2,1)}), bf16[2048,768]{1,0:T(8,128)(2,1)}) %all-gather.12.cloned.1.call-update) | async-done | bytes 3145744 | tf_op jit(solution)/shard_map/all_gather | solution.py:57
  161.7 77.2 %all-gather.16.cloned.1.call-done = bf16[768,2048]{1,0:T(8,128)(2,1)} async-done(((bf16[768,128]{1,0:T(8,128)(2,1)}), bf16[768,2048]{1,0:T(8,128)(2,1)}) %all-gather.16.cloned.1.call-update) | async-done | bytes 3145744 | tf_op jit(solution)/shard_map/all_gather | solution.py:84
  238.9 6.2 fusion.3
  245.1 0.0 all-reduce.2.cloned.1.call-update
  245.1 0.0 all-gather.18.cloned.1.call-start
  245.2 0.0 copy-done.1
  245.2 1.0 convert_element_type.74
  246.1 0.0 all-gather.18.cloned.1.call-update
  246.2 0.0 copy-start.7
  246.2 0.0 all-gather.20.cloned.1.call-start
  246.2 2.4 convert_element_type.75
  248.6 0.0 all-gather.20.cloned.1.call-update
  248.6 0.0 copy-start.8
  248.7 0.0 copy-start.11
  248.7 0.0 all-gather.22.cloned.1.call-start
  248.7 0.9 convert_element_type.77
  249.7 0.0 all-gather.22.cloned.1.call-update
  249.7 0.0 reduce-scatter.2.cloned.1.call-start
  249.8 38.3 %all-gather.1 = f32[16,1,128]{2,1,0:T(1,128)S(1)} all-gather(f32[1,1,128]{2,1,0:T(1,128)S(1)} %bitcast.35), channel_id=1, replica_groups=mesh['fs'=16,'tp'=2] {'fs'}, dimensions={0}, use_global_device_ids=true | all-gather | bytes 8704 | tf_op jit(solution)/shard_map/all_gather | solution.py:48
  288.0 1.7 fusion.4
  289.8 118.3 %all-gather.18.cloned.1.call-done = bf16[2048,2816]{1,0:T(8,128)(2,1)} async-done(((bf16[128,2816]{1,0:T(8,128)(2,1)}), bf16[2048,2816]{1,0:T(8,128)(2,1)}) %all-gather.18.cloned.1.call-update) | async-done | bytes 11534352 | tf_op jit(solution)/shard_map/all_gather | solution.py:93
  408.1 0.0 copy-done.8
  408.1 9.1 %convolution_multiply_fusion.1 = f32[256,2816]{1,0:T(8,128)} fusion(bf16[2048,2816]{1,0:T(8,128)(2,1)} %all-gather.18.cloned.1.call-done, f32[2816]{0:T(1024)S(1)} %copy-done.8, bf16[256,2048]{1,0:T(8,128)(2,1)S(1)} %get-tuple-element.6, f32[2048]{0:T(1024)S(1)} %copy-done.11, f32[256]{0:T(256)S(1)} %add_rsqrt_fusion), kind=kOutput, calls=%fused_computation.2 | convolution fusion | flops 2955608064 | bytes 15486976 | tf_op jit(solution)/shard_map/dot_general | solution.py:96
  417.3 133.3 %all-gather.20.cloned.1.call-done = bf16[2048,2816]{1,0:T(8,128)(2,1)} async-done(((bf16[128,2816]{1,0:T(8,128)(2,1)}), bf16[2048,2816]{1,0:T(8,128)(2,1)}) %all-gather.20.cloned.1.call-update) | async-done | bytes 11534352 | tf_op jit(solution)/shard_map/all_gather | solution.py:94
  550.5 183.0 %all-gather.22.cloned.1.call-done = bf16[2816,2048]{1,0:T(8,128)(2,1)} async-done(((bf16[2816,128]{1,0:T(8,128)(2,1)}), bf16[2816,2048]{1,0:T(8,128)(2,1)}) %all-gather.22.cloned.1.call-update) | async-done | bytes 11534352 | tf_op jit(solution)/shard_map/all_gather | solution.py:104
  733.5 15.7 %fusion.2 = bf16[256,2048]{1,0:T(8,128)(2,1)} fusion(bf16[2816,2048]{1,0:T(8,128)(2,1)} %all-gather.22.cloned.1.call-done, f32[2048]{0:T(1024)S(1)} %bitcast.33, bf16[2048,2816]{1,0:T(8,128)(2,1)} %all-gather.20.cloned.1.call-done, f32[256,2816]{1,0:T(8,128)} %convolution_multiply_fusion.1, f32[2816]{0:T(1024)S(1)} %copy-done.9, ...), kind=kOutput, calls=%fused_computation.11 | convolution fusion | flops 5913772032 | bytes 28078080 | tf_op jit(solution)/shard_map/dot_general | solution.py:23
  749.2 0.0 reduce-scatter.2.cloned.1.call-update
  749.2 6.7 reduce-scatter.2.cloned.1.call-done
  755.9 2.0 add_convert_fusion
  (18 shorter events, 0.1 us)
Async XLA Ops:
  6.5 6.1 copy-start.6
  6.5 86.0 %copy-start.10 = (f32[2048]{0:T(1024)S(1)}, f32[2048]{0:T(1024)}, u32[]{:S(2)}) copy-start(f32[2048]{0:T(1024)} %param.19) | copy-start | bytes 24580
  6.5 86.0 %copy-start.12 = (f32[768]{0:T(1024)S(1)}, f32[768]{0:T(1024)}, u32[]{:S(2)}) copy-start(f32[768]{0:T(1024)} %param.23) | copy-start | bytes 9220
  6.5 48.6 %all-gather.10.cloned.1.call-start = ((), (), s32[]{:S(2)}) async-start(), calls=%async_computation.1 | async-start | bytes 1572864 | tf_op jit(solution)/shard_map/all_gather | solution.py:50
  7.3 85.3 %all-gather.14.cloned.1.call-start = ((), (), s32[]{:S(2)}) async-start(), calls=%async_computation.3 | async-start | bytes 3342336 | tf_op jit(solution)/shard_map/all_gather | solution.py:58
  9.0 152.7 %all-gather.12.cloned.1.call-start = ((), (), s32[]{:S(2)}) async-start(), calls=%async_computation.2 | async-start | bytes 3342336 | tf_op jit(solution)/shard_map/all_gather | solution.py:57
  10.8 228.1 %all-gather.16.cloned.1.call-start = ((), (), s32[]{:S(2)}) async-start(), calls=%async_computation.4 | async-start | bytes 3342336 | tf_op jit(solution)/shard_map/all_gather | solution.py:84
  12.6 275.5 %all-reduce.2.cloned.1.call-start = ((), (), s32[]{:S(2)}) async-start(), calls=%async_computation.5 | async-start | bytes 2097152 | tf_op jit(solution)/shard_map/psum | solution.py:86
  56.7 42.0 %copy-start.5 = (f32[768]{0:T(1024)S(1)}, f32[768]{0:T(1024)}, u32[]{:S(2)}) copy-start(f32[768]{0:T(1024)} %param.24) | copy-start | bytes 9220
  56.7 42.4 %copy-start.4 = (f32[12,128]{1,0:T(8,128)S(1)}, f32[12,128]{1,0:T(8,128)}, u32[]{:S(2)}) copy-start(f32[12,128]{1,0:T(8,128)} %param.26) | copy-start | bytes 18436
  96.0 3.1 copy-start.3
  99.1 139.8 %copy-start = (bf16[256,2048]{1,0:T(8,128)(2,1)S(1)}, bf16[256,2048]{1,0:T(8,128)(2,1)}, u32[]{:S(2)}) copy-start(bf16[256,2048]{1,0:T(8,128)(2,1)} %all-gather.10.cloned.1.call-done) | copy-start | bytes 3145732
  99.1 139.8 %copy-start.13 = (f32[768]{0:T(1024)S(1)}, f32[768]{0:T(1024)}, u32[]{:S(2)}) copy-start(f32[768]{0:T(1024)} %param.21) | copy-start | bytes 9220
  238.9 6.2 copy-start.1
  245.1 163.0 %all-gather.18.cloned.1.call-start = ((), (), s32[]{:S(2)}) async-start(), calls=%async_computation.6 | async-start | bytes 12255232 | tf_op jit(solution)/shard_map/all_gather | solution.py:93
  246.1 2.6 copy-start.2
  246.2 3.6 copy-start.7
  246.2 304.4 %all-gather.20.cloned.1.call-start = ((), (), s32[]{:S(2)}) async-start(), calls=%async_computation.7 | async-start | bytes 12255232 | tf_op jit(solution)/shard_map/all_gather | solution.py:94
  248.6 159.5 %copy-start.8 = (f32[2816]{0:T(1024)S(1)}, f32[2816]{0:T(1024)}, u32[]{:S(2)}) copy-start(f32[2816]{0:T(1024)} %param.31) | copy-start | bytes 33796
  248.7 159.5 %copy-start.11 = (f32[2048]{0:T(1024)S(1)}, f32[2048]{0:T(1024)}, u32[]{:S(2)}) copy-start(f32[2048]{0:T(1024)} %param.29) | copy-start | bytes 24580
  248.7 484.8 %all-gather.22.cloned.1.call-start = ((), (), s32[]{:S(2)}) async-start(), calls=%async_computation.8 | async-start | bytes 12255232 | tf_op jit(solution)/shard_map/all_gather | solution.py:104
  249.7 506.2 %reduce-scatter.2.cloned.1.call-start = ((), (), s32[]{:S(2)}) async-start(), calls=%async_computation.9 | async-start | bytes 1572864 | tf_op jit(solution)/shard_map/reduce_scatter | solution.py:106
  408.1 325.4 %copy-start.9 = (f32[2816]{0:T(1024)S(1)}, f32[2816]{0:T(1024)}, u32[]{:S(2)}) copy-start(f32[2816]{0:T(1024)} %param.33) | copy-start | bytes 33796
Sparse Core Ops, SparseCore 0:
  8.9 11.7 all-gather.9
  23.4 69.0 all-gather.13
  95.3 66.3 all-gather.11
  164.3 74.5 all-gather.15
  245.2 17.5 all-reduce.1
  265.5 142.6 all-gather.17
  410.9 139.6 all-gather.19
  553.2 180.2 all-gather.21
  749.3 6.5 reduce-scatter.1
where the time goes:
time: 765 us; the launch traced here: 764 us
  waiting for transfers between devices  616 us (81%)
  blocking collectives  83.3 us (11%)
  matrix products  34.8 us (5%)
  other arithmetic  14.9 us (2%)
  between operations  13.4 us (2%)
    all_gather x1, waiting for transfers between devices, on_device(): lax.all_gather(lowering_matrix.astype(jnp.bfloat16), 'fs', axis=1, tiled=...  183 us
    all_gather x1, waiting for transfers between devices, on_device(): lax.all_gather(up_half, 'fs', axis=0, tiled=True)  133 us
    all_gather x1, waiting for transfers between devices, on_device(): lax.all_gather(gate_half, 'fs', axis=0, tiled=True)  118 us
    all_gather x1, waiting for transfers between devices, on_device(): lax.all_gather(branch_emission_matrix.astype(jnp.bfloat16), 'fs', axis=1,...  77.2 us
    all_gather x1, waiting for transfers between devices, on_device(): lax.all_gather(conveyor_matrix.astype(jnp.bfloat16), 'fs', axis=0, tiled=...  61.3 us
    all_gather x1, blocking collectives, on_device(): lax.all_gather(emission_rescalers, 'fs', axis=0, tiled=True)  42.5 us
    all_gather x1, blocking collectives, on_device(): lax.all_gather(lowering_rescalers, 'fs', axis=0, tiled=True)  38.3 us
    all_gather x1, waiting for transfers between devices, on_device(): lax.all_gather(blend_value_matrix.astype(jnp.bfloat16), 'fs', axis=0, til...  35.8 us
  transfers between devices with their start and end apart: 9, of which 7 were waited for; matrix products, arithmetic and copies ran while one was open for 4% of the time, Pallas kernels for 0%

commit v1 on v0

--- a/solution.py
+++ b/solution.py
@@ -2,6 +2,7 @@
 import jax.numpy as jnp
 from jax import lax
 from jax.sharding import PartitionSpec as P
+from jax.lax import all_gather
 
 EPS = 1e-06
 
@@ -98,10 +99,13 @@
     hidden = (jax.nn.silu(pre_gate * valve_rescalers) * (pre_up * raising_rescalers)).astype(
         jnp.bfloat16
     )
+
+    def kinds_prepare(m, axis_id):
+        base_arr = jnp.concatenate(all_gather(m, axis_name=axis_id), 1)
+        return base_arr
+
     ffn_terms = project_cols(
-        hidden,
-        down_scales,
-        lax.all_gather(lowering_matrix.astype(jnp.bfloat16), "fs", axis=1, tiled=True),
+        hidden, down_scales, kinds_prepare(lowering_matrix.astype(jnp.bfloat16), "fs")
     )
     ffn_share = lax.psum_scatter(
         ffn_terms.astype(jnp.bfloat16), "tp", scatter_dimension=1, tiled=True

time: 765 us -> 725 us (0.948)
  waiting for transfers between devices: 616 us -> 561 us
  local copies, waits for them, and re-layouts: 1.27 us -> 16.4 us
    all_gather x1, waiting for transfers between devices: 183 us -> 118 us  [kinds_prepare(): base_arr = jnp.concatenate(all_gather(m, axis_name=axis_id), 1)]
    reshape x0 -> x1, local copies, waits for them, and re-layouts: none -> 15.2 us  [kinds_prepare(): base_arr = jnp.concatenate(all_gather(m, axis_name=axis_id), 1)]
    all_gather x1, waiting for transfers between devices: 118 us -> 127 us  [on_device(): lax.all_gather(gate_half, 'fs', axis=0, tiled=True)]
  transfers between devices with their start and end apart: 9 -> 9, of which waited for: 7 -> 7; matrix products, arithmetic and copies ran while one was open for 4% -> 6% of each run, Pallas kernels for 0% -> 0%
where the time goes in v1:
time: 725 us; the launch traced here: 724 us
  waiting for transfers between devices  561 us (77%)
  blocking collectives  83.3 us (11%)
  matrix products  34.8 us (5%)
  local copies, waits for them, and re-layouts  16.4 us (2%)
  other arithmetic  14.9 us (2%)
  between operations  13.4 us (2%)
    all_gather x1, waiting for transfers between devices, on_device(): lax.all_gather(up_half, 'fs', axis=0, tiled=True)  133 us
    all_gather x1, waiting for transfers between devices, on_device(): lax.all_gather(gate_half, 'fs', axis=0, tiled=True)  127 us
    all_gather x1, waiting for transfers between devices, kinds_prepare(): base_arr = jnp.concatenate(all_gather(m, axis_name=axis_id), 1)  118 us
    all_gather x1, waiting for transfers between devices, on_device(): lax.all_gather(branch_emission_matrix.astype(jnp.bfloat16), 'fs', axis=1,...  77.2 us
    all_gather x1, waiting for transfers between devices, on_device(): lax.all_gather(conveyor_matrix.astype(jnp.bfloat16), 'fs', axis=0, tiled=...  61.3 us
    all_gather x1, blocking collectives, on_device(): lax.all_gather(emission_rescalers, 'fs', axis=0, tiled=True)  42.5 us
    all_gather x1, blocking collectives, on_device(): lax.all_gather(lowering_rescalers, 'fs', axis=0, tiled=True)  38.3 us
    all_gather x1, waiting for transfers between devices, on_device(): lax.all_gather(blend_value_matrix.astype(jnp.bfloat16), 'fs', axis=0, til...  35.8 us
  transfers between devices with their start and end apart: 9, of which 7 were waited for; matrix products, arithmetic and copies ran while one was open for 6% of the time, Pallas kernels for 0%

profile of v1, /device:TPU:0, one launch (start us, length us, event | category | flops | bytes accessed | tf_op | source)
XLA Modules:
  0.0 723.9 jit_solution(17273863778185249813)
XLA Ops:
  6.5 0.0 all-gather.11.cloned.1.call-start
  6.5 0.7 all-gather.11.cloned.1.call-update
  7.3 0.0 all-gather.15.cloned.1.call-start
  7.3 1.7 convert_element_type.64
  9.0 0.0 all-gather.15.cloned.1.call-update
  9.0 0.0 all-gather.13.cloned.1.call-start
  9.1 1.7 convert_element_type.63
  10.8 0.0 all-gather.13.cloned.1.call-update
  10.8 0.0 all-gather.17.cloned.1.call-start
  10.9 1.7 convert_element_type.67
  12.5 0.0 all-gather.17.cloned.1.call-update
  12.6 0.0 all-reduce.2.cloned.1.call-start
  12.6 0.0 copy-done.6
  12.6 42.5 %all-gather.1 = f32[16,1,128]{2,1,0:T(1,128)S(1)} all-gather(f32[1,1,128]{2,1,0:T(1,128)S(1)} %bitcast.40), channel_id=1, replica_groups=mesh['fs'=16,'tp'=2] {'fs'}, dimensions={0}, use_global_device_ids=true | all-gather | bytes 8704 | tf_op jit(solution)/shard_map/all_gather | solution.py:48
  55.1 0.0 all-gather.11.cloned.1.call-done
  55.1 1.5 fusion.7
  56.7 0.0 copy-start.5
  56.7 0.0 copy-start.4
  56.7 35.8 %all-gather.15.cloned.1.call-done = bf16[2048,768]{1,0:T(8,128)(2,1)} async-done(((bf16[128,768]{1,0:T(8,128)(2,1)}), bf16[2048,768]{1,0:T(8,128)(2,1)}) %all-gather.15.cloned.1.call-update) | async-done | bytes 3145744 | tf_op jit(solution)/shard_map/all_gather | solution.py:59
  92.5 0.0 copy-done.10
  92.5 0.0 copy-done.12
  92.5 3.5 multiply_reduce_fusion
  96.0 0.0 copy-start.3
  96.0 2.6 psum.14
  98.6 0.0 copy-done.5
  98.6 0.1 multiply_convert_fusion
  98.8 0.2 copy.30
  99.0 0.1 reshape.46
  99.1 0.0 copy-done.4
  99.1 0.0 copy-done.3
  99.1 0.0 copy-start
  99.1 0.0 copy-start.13
  99.1 0.4 fusion.11
  99.5 0.6 copy.32
  100.1 0.1 copy.40
  100.2 0.3 copy.33
  100.4 61.3 %all-gather.13.cloned.1.call-done = bf16[2048,768]{1,0:T(8,128)(2,1)} async-done(((bf16[128,768]{1,0:T(8,128)(2,1)}), bf16[2048,768]{1,0:T(8,128)(2,1)}) %all-gather.13.cloned.1.call-update) | async-done | bytes 3145744 | tf_op jit(solution)/shard_map/all_gather | solution.py:58
  161.7 77.2 %all-gather.17.cloned.1.call-done = bf16[768,2048]{1,0:T(8,128)(2,1)} async-done(((bf16[768,128]{1,0:T(8,128)(2,1)}), bf16[768,2048]{1,0:T(8,128)(2,1)}) %all-gather.17.cloned.1.call-update) | async-done | bytes 3145744 | tf_op jit(solution)/shard_map/all_gather | solution.py:85
  238.9 6.2 fusion.3
  245.1 0.0 all-reduce.2.cloned.1.call-update
  245.1 0.0 all-gather.23.cloned.1.call-start
  245.2 0.0 copy-done.1
  245.2 1.0 convert_element_type.77
  246.1 0.0 all-gather.23.cloned.1.call-update
  246.2 0.0 copy-start.7
  246.2 0.0 all-gather.19.cloned.1.call-start
  246.2 2.4 convert_element_type.74
  248.6 0.0 all-gather.19.cloned.1.call-update
  248.7 0.0 all-gather.21.cloned.1.call-start
  248.7 0.9 convert_element_type.75
  249.7 0.0 all-gather.21.cloned.1.call-update
  249.7 0.0 reduce-scatter.2.cloned.1.call-start
  249.7 0.0 copy-done.7
  249.7 38.3 %all-gather.2 = f32[16,1,128]{2,1,0:T(1,128)S(1)} all-gather(f32[1,1,128]{2,1,0:T(1,128)S(1)} %bitcast.41), channel_id=1, replica_groups=mesh['fs'=16,'tp'=2] {'fs'}, dimensions={0}, use_global_device_ids=true | all-gather | bytes 8704 | tf_op jit(solution)/shard_map/all_gather | solution.py:49
  288.0 1.7 fusion.4
  289.8 118.3 %all-gather.23.cloned.1.call-done = bf16[45056,128]{1,0:T(8,128)(2,1)} async-done(((bf16[2816,128]{1,0:T(8,128)(2,1)}), bf16[45056,128]{1,0:T(8,128)(2,1)}) %all-gather.23.cloned.1.call-update) | async-done | bytes 11534352 | tf_op jit(solution)/shard_map/all_gather | solution.py:104
  408.1 15.2 %copy.34 = bf16[2816,16,128]{0,2,1:T(8,128)(2,1)} copy(bf16[2816,16,128]{2,0,1:T(8,128)(2,1)} %bitcast.33) | data formatting | bytes 23068672 | tf_op jit(solution)/shard_map/reshape | solution.py:104
  423.3 127.2 %all-gather.19.cloned.1.call-done = bf16[2048,2816]{1,0:T(8,128)(2,1)} async-done(((bf16[128,2816]{1,0:T(8,128)(2,1)}), bf16[2048,2816]{1,0:T(8,128)(2,1)}) %all-gather.19.cloned.1.call-update) | async-done | bytes 11534352 | tf_op jit(solution)/shard_map/all_gather | solution.py:94
  550.5 9.1 %convolution_multiply_fusion.1 = f32[256,2816]{1,0:T(8,128)} fusion(bf16[2048,2816]{1,0:T(8,128)(2,1)} %all-gather.19.cloned.1.call-done, f32[2816]{0:T(1024)S(1)} %copy-done.8, bf16[256,2048]{1,0:T(8,128)(2,1)S(1)} %get-tuple-element.6, f32[2048]{0:T(1024)S(1)} %copy-done.11, f32[256]{0:T(256)S(1)} %add_rsqrt_fusion), kind=kOutput, calls=%fused_computation.2 | convolution fusion | flops 2955608064 | bytes 15486976 | tf_op jit(solution)/shard_map/dot_general | solution.py:97
  559.6 133.3 %all-gather.21.cloned.1.call-done = bf16[2048,2816]{1,0:T(8,128)(2,1)} async-done(((bf16[128,2816]{1,0:T(8,128)(2,1)}), bf16[2048,2816]{1,0:T(8,128)(2,1)}) %all-gather.21.cloned.1.call-update) | async-done | bytes 11534352 | tf_op jit(solution)/shard_map/all_gather | solution.py:95
  692.9 15.7 %fusion.2 = bf16[256,2048]{1,0:T(8,128)(2,1)} fusion(bf16[2816,2048]{0,1:T(8,128)(2,1)} %bitcast.34, f32[2048]{0:T(1024)S(1)} %bitcast.39, bf16[2048,2816]{1,0:T(8,128)(2,1)} %all-gather.21.cloned.1.call-done, f32[256,2816]{1,0:T(8,128)} %convolution_multiply_fusion.1, f32[2816]{0:T(1024)S(1)} %copy-done.9, bf16[256,2048]{1,0:T(8,128)(2,1)S(1)} %get-tuple-element.6, ...), kind=kOutput, calls=%fused_computation.11 | convolution fusion | flops 5913772032 | bytes 28078080 | tf_op jit(solution)/shard_map/dot_general | solution.py:24
  708.6 0.0 reduce-scatter.2.cloned.1.call-update
  708.6 6.7 reduce-scatter.2.cloned.1.call-done
  715.3 2.0 add_convert_fusion
  (19 shorter events, 0.1 us)
Async XLA Ops:
  6.5 6.1 copy-start.6
  6.5 86.0 %copy-start.10 = (f32[2048]{0:T(1024)S(1)}, f32[2048]{0:T(1024)}, u32[]{:S(2)}) copy-start(f32[2048]{0:T(1024)} %param.19) | copy-start | bytes 24580
  6.5 86.0 %copy-start.12 = (f32[768]{0:T(1024)S(1)}, f32[768]{0:T(1024)}, u32[]{:S(2)}) copy-start(f32[768]{0:T(1024)} %param.23) | copy-start | bytes 9220
  6.5 48.6 %all-gather.11.cloned.1.call-start = ((), (), s32[]{:S(2)}) async-start(), calls=%async_computation.1 | async-start | bytes 1572864 | tf_op jit(solution)/shard_map/all_gather | solution.py:51
  7.3 85.3 %all-gather.15.cloned.1.call-start = ((), (), s32[]{:S(2)}) async-start(), calls=%async_computation.3 | async-start | bytes 3342336 | tf_op jit(solution)/shard_map/all_gather | solution.py:59
  9.0 152.7 %all-gather.13.cloned.1.call-start = ((), (), s32[]{:S(2)}) async-start(), calls=%async_computation.2 | async-start | bytes 3342336 | tf_op jit(solution)/shard_map/all_gather | solution.py:58
  10.8 228.1 %all-gather.17.cloned.1.call-start = ((), (), s32[]{:S(2)}) async-start(), calls=%async_computation.4 | async-start | bytes 3342336 | tf_op jit(solution)/shard_map/all_gather | solution.py:85
  12.6 275.5 %all-reduce.2.cloned.1.call-start = ((), (), s32[]{:S(2)}) async-start(), calls=%async_computation.5 | async-start | bytes 2097152 | tf_op jit(solution)/shard_map/psum | solution.py:87
  56.7 42.0 %copy-start.5 = (f32[768]{0:T(1024)S(1)}, f32[768]{0:T(1024)}, u32[]{:S(2)}) copy-start(f32[768]{0:T(1024)} %param.24) | copy-start | bytes 9220
  56.7 42.4 %copy-start.4 = (f32[12,128]{1,0:T(8,128)S(1)}, f32[12,128]{1,0:T(8,128)}, u32[]{:S(2)}) copy-start(f32[12,128]{1,0:T(8,128)} %param.26) | copy-start | bytes 18436
  96.0 3.1 copy-start.3
  99.1 139.8 %copy-start = (bf16[256,2048]{1,0:T(8,128)(2,1)S(1)}, bf16[256,2048]{1,0:T(8,128)(2,1)}, u32[]{:S(2)}) copy-start(bf16[256,2048]{1,0:T(8,128)(2,1)} %all-gather.11.cloned.1.call-done) | copy-start | bytes 3145732
  99.1 139.8 %copy-start.13 = (f32[768]{0:T(1024)S(1)}, f32[768]{0:T(1024)}, u32[]{:S(2)}) copy-start(f32[768]{0:T(1024)} %param.21) | copy-start | bytes 9220
  238.9 6.2 copy-start.1
  245.1 163.0 %all-gather.23.cloned.1.call-start = ((), (), s32[]{:S(2)}) async-start(), calls=%async_computation.9 | async-start | bytes 12255232 | tf_op jit(solution)/shard_map/all_gather | solution.py:104
  246.1 2.6 copy-start.2
  246.2 3.6 copy-start.7
  246.2 304.3 %all-gather.19.cloned.1.call-start = ((), (), s32[]{:S(2)}) async-start(), calls=%async_computation.6 | async-start | bytes 12255232 | tf_op jit(solution)/shard_map/all_gather | solution.py:94
  248.7 444.3 %all-gather.21.cloned.1.call-start = ((), (), s32[]{:S(2)}) async-start(), calls=%async_computation.7 | async-start | bytes 12255232 | tf_op jit(solution)/shard_map/all_gather | solution.py:95
  249.7 465.6 %reduce-scatter.2.cloned.1.call-start = ((), (), s32[]{:S(2)}) async-start(), calls=%async_computation.8 | async-start | bytes 1572864 | tf_op jit(solution)/shard_map/reduce_scatter | solution.py:110
  408.1 142.4 %copy-start.8 = (f32[2816]{0:T(1024)S(1)}, f32[2816]{0:T(1024)}, u32[]{:S(2)}) copy-start(f32[2816]{0:T(1024)} %param.31) | copy-start | bytes 33796
  408.1 142.4 %copy-start.11 = (f32[2048]{0:T(1024)S(1)}, f32[2048]{0:T(1024)}, u32[]{:S(2)}) copy-start(f32[2048]{0:T(1024)} %param.29) | copy-start | bytes 24580
  550.5 142.4 %copy-start.9 = (f32[2816]{0:T(1024)S(1)}, f32[2816]{0:T(1024)}, u32[]{:S(2)}) copy-start(f32[2816]{0:T(1024)} %param.33) | copy-start | bytes 33796
Sparse Core Ops, SparseCore 0:
  8.9 11.7 all-gather.10
  23.4 69.0 all-gather.14
  95.3 66.3 all-gather.12
  164.3 74.5 all-gather.16
  245.2 17.5 all-reduce.1
  265.5 142.6 all-gather.22
  410.9 139.5 all-gather.18
  553.3 139.6 all-gather.20
  708.7 6.5 reduce-scatter.1
